TPU v7x, 128 devices: a whole 4x4x4 slice. The times are simulated.
128 devices in a mesh: fs: 16 (over z, x), tp: 8 (over y, core).
Axes of the slice: x: 4, y: 4, z: 4, core: 2. Of those that a mesh axis runs over, the one named last changes fastest.
Arguments:
- h_saved: bfloat16 [32768, 2048], P('fs'), may hold values from -6 to 6
- conv_cotan: bfloat16 [32768, 2560], P('fs', 'tp'), may hold values from -64 to 64
- lru_out: bfloat16 [32768, 2560], P('fs', 'tp'), may hold values from -64 to 64
- out_cotan: bfloat16 [32768, 2048], P('fs'), may hold values from -6 to 6
- basis_in: bfloat16 [2048, 256], P('fs'), may hold values from -1.41421356 to 1.41421356
- basis_out: bfloat16 [2048, 256], P('fs'), may hold values from -1.41421356 to 1.41421356
- weight_in: float32 [2048, 2560], P('fs', 'tp'), may hold values from -0.125 to 0.125
- weight_out: float32 [2560, 2048], P('tp', 'fs'), may hold values from -0.125 to 0.125
- first_in: float32 [256, 2560], P('fs', 'tp'), may hold values from -6 to 6
- second_in: float32 [256, 2560], P('fs', 'tp'), may hold values from 0.05 to 2
- first_out: float32 [256, 2560], P('fs', 'tp'), may hold values from -6 to 6
- second_out: float32 [256, 2560], P('fs', 'tp'), may hold values from 0.05 to 2
Outputs:
- step_in: float32 [2048, 2560], P('fs', 'tp')
- new_weight_in: float32 [2048, 2560], P('fs', 'tp')
- copy_in: bfloat16 [2048, 2560], P(None, 'tp')
- new_first_in: float32 [256, 2560], P('fs', 'tp')
- new_second_in: float32 [256, 2560], P('fs', 'tp')
- step_out: float32 [2560, 2048], P('tp', 'fs')
- new_weight_out: float32 [2560, 2048], P('tp', 'fs')
- copy_out: bfloat16 [2560, 2048], P('tp')
- new_first_out: float32 [256, 2560], P('fs', 'tp')
- new_second_out: float32 [256, 2560], P('fs', 'tp')
All inputs are finite; a program needn't handle non-finite values.
Results may differ from a plain program's by a relative error of at most 0.0046.
Values may be sent and summed in bfloat16 or wider, within the bound.
No kernel may reach another device: no remote copies, remote signals or barrier semaphores. Data moves between devices by JAX's collectives and lax.ppermute only.
A program may use at most 128 MiB of HBM per device.

v0:
```python
import math
import jax
import jax.numpy as jnp
from jax import lax
from jax.sharding import Mesh
from jax.sharding import PartitionSpec as P

D_RNN = 2560
RANK = 256
FS = ("fs_0", "fs_1")
FS_TP = ("fs_0", "fs_1", "tp_0", "tp_1")
TP = ("tp_0", "tp_1")


def laid_out(blocks, dim):
    blocks = jnp.moveaxis(blocks, 0, dim)
    lengths = blocks.shape
    return blocks.reshape(*lengths[:dim], lengths[dim] * lengths[dim + 1], *lengths[dim + 2 :])


def sent_to_all(array, axis):
    copies = jnp.broadcast_to(array, (lax.axis_size(axis), *array.shape))
    return lax.all_to_all(copies, axis, split_axis=0, concat_axis=0, tiled=True)


def gather_directly(array, axis, dim):
    return laid_out(sent_to_all(array, axis), dim)


def in_one_piece(arrays, axis, dim, along):
    ends, at = ([], 0)
    for a in arrays[:-1]:
        at += a.shape[along]
        ends.append(at)
    both = jnp.concatenate(arrays, axis=along)
    return tuple(jnp.split(gather_directly(both, axis, dim), ends, axis=along))


def split_up(array, dim, size):
    lengths = array.shape
    blocks = array.reshape(*lengths[:dim], size, lengths[dim] // size, *lengths[dim + 1 :])
    return jnp.moveaxis(blocks, dim, 0)


def sent_and_summed(array, axis, dim):
    blocks = split_up(array, dim, lax.axis_size(axis))
    arrived = lax.all_to_all(blocks, axis, split_axis=0, concat_axis=0, tiled=True)
    return arrived.sum(axis=0)


def sent_together(arrays, axis, dim, along):
    both = jnp.concatenate(arrays, axis=along)
    filled, at, done = (sent_and_summed(both, axis, dim), 0, [])
    for a in arrays:
        done.append(lax.slice_in_dim(filled, at, at + a.shape[along], axis=along))
        at += a.shape[along]
    return tuple(done)


def by_axis(array, axes):
    for axis in axes:
        array = lax.psum(array, axis)
    return array


def in_one_piece_2(arrays, axis, dim, along):
    widths = [a.shape[along] for a in arrays]
    both = jnp.concatenate(arrays, axis=along)
    filled = lax.all_gather(both, axis, axis=dim, tiled=True)
    return tuple(jnp.split(filled, [sum(widths[:k]) for k in range(1, len(widths))], axis=along))


def turned_gather(arrays, axis, dims):
    turned = [jnp.moveaxis(a, dim, 0) for a, dim in zip(arrays, dims)]
    widths = [t[0].size for t in turned]
    both = jnp.concatenate([t.reshape(-1, w) for t, w in zip(turned, widths)], axis=1)
    filled = lax.all_gather(both, axis, axis=0, tiled=True)
    blocks = jnp.split(filled, [sum(widths[:k]) for k in range(1, len(widths))], axis=1)
    return tuple(
        (
            jnp.moveaxis(b.reshape(-1, *t.shape[1:]), 0, dim)
            for b, t, dim in zip(blocks, turned, dims)
        )
    )


def split_product(narrow, wide):
    upper = lax.optimization_barrier(wide.astype(jnp.bfloat16))
    lower = (wide - upper.astype(jnp.float32)).astype(jnp.bfloat16)
    turned = jnp.transpose(narrow)
    first_part = jnp.dot(turned, upper, preferred_element_type=jnp.float32)
    second_part = jnp.dot(turned, lower, preferred_element_type=jnp.float32)
    return first_part + second_part


def moments(proj, factor, first, second):
    scaled = factor * proj
    first_new = 0.8 * first + 0.2 * scaled
    second_new = 0.9 * second + 0.1 * scaled * scaled
    direction = (first_new / (jnp.sqrt(second_new) + 1e-08)).astype(jnp.bfloat16)
    return (first_new, second_new, direction)


def shards(
    h_saved,
    conv_cotan,
    lru_out,
    out_cotan,
    basis_in,
    basis_out,
    weight_in,
    weight_out,
    first_in,
    second_in,
    first_out,
    second_out,
):
    pairs = ((h_saved, conv_cotan), (out_cotan, lru_out))
    partial_value = []
    wholes = in_one_piece((basis_in, basis_out), FS, 0, 1)
    for number in range(2):
        reduced = jnp.dot(pairs[number][0], wholes[number], preferred_element_type=jnp.float32)
        partial_value.append(split_product(pairs[number][1], reduced).T)
    proj_in, proj_out = sent_together((partial_value[0], partial_value[1]), FS, 0, 1)
    total = by_axis(jnp.sum(proj_in * proj_in) + jnp.sum(proj_out * proj_out), FS_TP)
    factor = math.sqrt(2.0 * RANK * D_RNN) * lax.rsqrt(total + 1e-06)
    first_a, second_a, dir_in = moments(proj_in, factor, first_in, second_in)
    first_b, second_b, dir_out = moments(proj_out, factor, first_out, second_out)
    full_in, full_out = in_one_piece_2((dir_in, dir_out), FS, 0, 1)
    step_in = jnp.dot(basis_in, full_in, preferred_element_type=jnp.float32)
    step_out = jnp.dot(basis_out, full_out, preferred_element_type=jnp.float32).T
    new_in = weight_in - 0.02 * step_in
    new_out = weight_out - 0.02 * step_out
    copy_in, copy_out = turned_gather(
        (new_in.astype(jnp.bfloat16), new_out.astype(jnp.bfloat16)), FS, (0, 1)
    )
    return (
        step_in,
        new_in,
        copy_in,
        first_a,
        second_a,
        step_out,
        new_out,
        copy_out,
        first_b,
        second_b,
    )


def solution(mesh):
    finer = Mesh(mesh.devices.reshape(4, 4, 4, 2), ("fs_0", "fs_1", "tp_0", "tp_1"))
    placed = (
        P(FS, None),
        P(FS, TP),
        P(FS, TP),
        P(FS, None),
        P(FS, None),
        P(FS, None),
        P(FS, TP),
        P(TP, FS),
        P(FS, TP),
        P(FS, TP),
        P(FS, TP),
        P(FS, TP),
    )
    return jax.shard_map(
        shards,
        mesh=finer,
        in_specs=placed,
        out_specs=(
            P(FS, TP),
            P(FS, TP),
            P(None, TP),
            P(FS, TP),
            P(FS, TP),
            P(TP, FS),
            P(TP, FS),
            P(TP, None),
            P(FS, TP),
            P(FS, TP),
        ),
        check_vma=False,
    )
```

profile of v0, /device:TPU:0, one launch (start us, length us, event | category | flops | bytes accessed | tf_op | source)
XLA Modules:
  0.0 189.7 jit_solution(8411399123699626168)
XLA Ops:
  7.2 1.0 pad_maximum_fusion.2
  8.4 36.4 %all_to_all.10 = bf16[16,128,512]{2,1,0:T(8,128)(2,1)S(1)} all-to-all(bf16[16,128,512]{2,1,0:T(8,128)(2,1)S(1)} %broadcast_in_dim.3), channel_id=1, replica_groups=mesh['fs_0'=4,'fs_1'=4,'tp_0'=4,'tp_1'=2] {'fs_0','fs_1'}, dimensions={0} | all-to-all | bytes 4194304 | tf_op jit(solution)/shard_map/all_to_all | solution.py:23
  44.9 5.9 %fusion.10 = (bf16[2048,256]{0,1:T(8,128)(2,1)S(1)}, f32[2048,256]{0,1:T(8,128)S(1)}) fusion(bf16[2048,2048]{1,0:T(8,128)(2,1)} %param.15, bf16[2048,512]{1,0:T(8,128)(2,1)S(1)} %bitcast.23), kind=kOutput, calls=%fused_computation.33 | convolution fusion | flops 2148007936 | bytes 12582912 | tf_op jit(solution)/shard_map/dot_general | solution.py:122
  50.8 2.4 %fusion.11 = (bf16[2048,256]{0,1:T(8,128)(2,1)S(1)}, f32[2048,256]{0,1:T(8,128)S(1)}) fusion(bf16[2048,2048]{1,0:T(8,128)(2,1)S(1)} %bitcast.26, bf16[2048,512]{1,0:T(8,128)(2,1)S(1)} %bitcast.24), kind=kOutput, calls=%fused_computation.34 | convolution fusion | flops 2148007936 | bytes 12582912 | tf_op jit(solution)/shard_map/dot_general | solution.py:122
  53.2 0.5 fusion.13
  53.8 0.6 convolution_add_fusion
  54.4 0.7 copy-done.1
  55.1 0.5 fusion.12
  55.6 0.6 convolution_add_fusion.1
  56.4 0.2 copy.22
  56.6 15.2 %all_to_all.11 = f32[16,16,640]{2,1,0:T(8,128)S(1)} all-to-all(f32[16,16,640]{2,1,0:T(8,128)S(1)} %bitcast.22), channel_id=1, replica_groups=mesh['fs_0'=4,'fs_1'=4,'tp_0'=4,'tp_1'=2] {'fs_0','fs_1'}, dimensions={0} | all-to-all | bytes 1310720 | tf_op jit(solution)/shard_map/all_to_all | solution.py:47
  71.9 0.7 multiply_reduce_fusion
  73.9 9.1 %psum.28 = f32[]{:T(128)} all-reduce(f32[]{:T(128)S(6)} %add.42), channel_id=1, replica_groups=mesh['fs_0'=4,'fs_1'=4,'tp_0'=4,'tp_1'=2] {'fs_0'}, use_global_device_ids=true, to_apply=%region_3.0 | all-reduce | flops 1 | bytes 8 | tf_op jit(solution)/shard_map/psum | solution.py:62
  83.0 9.6 %psum.29 = f32[]{:T(128)} all-reduce(f32[]{:T(128)} %psum.28), channel_id=1, replica_groups=mesh['fs_0'=4,'fs_1'=4,'tp_0'=4,'tp_1'=2] {'fs_1'}, use_global_device_ids=true, to_apply=%region_4.0 | all-reduce | flops 1 | bytes 8 | tf_op jit(solution)/shard_map/psum | solution.py:62
  92.6 11.4 %psum.30 = f32[]{:T(128)} all-reduce(f32[]{:T(128)} %psum.29), channel_id=1, replica_groups=mesh['fs_0'=4,'fs_1'=4,'tp_0'=4,'tp_1'=2] {'tp_0'}, use_global_device_ids=true, to_apply=%region_5.0 | all-reduce | flops 1 | bytes 8 | tf_op jit(solution)/shard_map/psum | solution.py:62
  103.9 3.1 %psum.31 = f32[]{:T(128)} all-reduce(f32[]{:T(128)} %psum.30), channel_id=1, replica_groups=mesh['fs_0'=4,'fs_1'=4,'tp_0'=4,'tp_1'=2] {'tp_1'}, use_global_device_ids=true, to_apply=%region_6.0 | all-reduce | flops 1 | bytes 8 | tf_op jit(solution)/shard_map/psum | solution.py:62
  107.8 0.7 divide_convert_fusion.1
  108.5 21.7 %all_gather.6 = bf16[256,640]{1,0:T(8,128)(2,1)S(1)} all-gather(bf16[16,640]{1,0:T(8,128)(2,1)S(1)} %pad_maximum_fusion.3), channel_id=1, replica_groups=mesh['fs_0'=4,'fs_1'=4,'tp_0'=4,'tp_1'=2] {'fs_0','fs_1'}, dimensions={0}, use_global_device_ids=true | all-gather | bytes 348160 | tf_op jit(solution)/shard_map/all_gather | solution.py:69
  130.2 0.3 fusion.2
  130.6 1.0 fusion.7
  131.5 0.7 convert_bitcast_fusion
  132.2 0.7 pad_maximum_fusion.1
  132.9 46.4 %all-gather.2.cloned.1.call-done = bf16[2048,640]{0,1:T(8,128)(2,1)} async-done(((bf16[128,640]{0,1:T(8,128)(2,1)}), bf16[2048,640]{0,1:T(8,128)(2,1)}) %all-gather.2.cloned.1.call-update) | async-done | bytes 2621456 | tf_op jit(solution)/shard_map/all_gather | solution.py:77
  179.4 3.5 %slice_bitcast_fusion = (bf16[320,2048]{1,0:T(8,128)(2,1)}, bf16[2048,320]{0,1:T(8,128)(2,1)}) fusion(bf16[2048,640]{0,1:T(8,128)(2,1)} %all-gather.2.cloned.1.call-done), kind=kLoop, calls=%fused_computation.4 | loop fusion | bytes 5242880 | tf_op jit(solution)/shard_map/transpose | solution.py:81
  (32 shorter events, 0.5 us)
Async XLA Ops:
  7.2 46.1 %copy-start = (bf16[2048,320]{0,1:T(8,128)(2,1)S(1)}, bf16[2048,320]{0,1:T(8,128)(2,1)}, u32[]{:S(2)}) copy-start(bf16[2048,320]{0,1:T(8,128)(2,1)} %param.14) | copy-start | bytes 3932164
  7.2 172.2 %all-gather.2.cloned.1.call-start = ((), (), s32[]{:S(2)}) async-start(), calls=%async_computation.2 | async-start | bytes 2785280 | tf_op jit(solution)/shard_map/all_gather | solution.py:77
  8.4 42.4 %slice-start = ((s8[8388608]{0:T(1024)(128)(4,1)}), s8[4194304]{0:T(1024)(128)(4,1)S(1)}, s32[]{:S(2)}) async-start(s8[8388608]{0:T(1024)(128)(4,1)} %bitcast.25), calls=%async_computation.3 | async-start | bytes 8388608
  44.9 5.9 %slice-start.1 = ((s8[8388608]{0:T(1024)(128)(4,1)}), s8[4194304]{0:T(1024)(128)(4,1)S(1)}, s32[]{:S(2)}) async-start(s8[8388608]{0:T(1024)(128)(4,1)} %bitcast.25), calls=%async_computation.4 | async-start | bytes 8388608
  53.8 1.3 copy-start.1
  56.2 51.5 %copy-start.7 = (f32[16,320]{1,0:T(8,128)S(1)}, f32[16,320]{1,0:T(8,128)}, u32[]{:S(2)}) copy-start(f32[16,320]{1,0:T(8,128)} %param.21) | copy-start | bytes 61444
  56.2 51.5 %copy-start.8 = (f32[16,320]{1,0:T(8,128)S(1)}, f32[16,320]{1,0:T(8,128)}, u32[]{:S(2)}) copy-start(f32[16,320]{1,0:T(8,128)} %param.20) | copy-start | bytes 61444
  56.3 51.5 %copy-start.9 = (f32[16,320]{1,0:T(8,128)S(1)}, f32[16,320]{1,0:T(8,128)}, u32[]{:S(2)}) copy-start(f32[16,320]{1,0:T(8,128)} %param.23) | copy-start | bytes 61444
  56.3 51.5 %copy-start.10 = (f32[16,320]{1,0:T(8,128)S(1)}, f32[16,320]{1,0:T(8,128)}, u32[]{:S(2)}) copy-start(f32[16,320]{1,0:T(8,128)} %param.22) | copy-start | bytes 61444
  56.3 73.9 %copy-start.4 = (bf16[128,256]{1,0:T(8,128)(2,1)S(1)}, bf16[128,256]{1,0:T(8,128)(2,1)}, u32[]{:S(2)}) copy-start(bf16[128,256]{1,0:T(8,128)(2,1)} %param.17) | copy-start | bytes 196612
  56.3 74.2 %copy-start.3 = (bf16[128,256]{1,0:T(8,128)(2,1)S(1)}, bf16[128,256]{1,0:T(8,128)(2,1)}, u32[]{:S(2)}) copy-start(bf16[128,256]{1,0:T(8,128)(2,1)} %param.16) | copy-start | bytes 196612
  56.4 74.2 %copy-start.5 = (f32[128,320]{0,1:T(8,128)S(1)}, f32[128,320]{0,1:T(8,128)}, u32[]{:S(2)}) copy-start(f32[128,320]{0,1:T(8,128)} %param.18) | copy-start | bytes 491524
  56.6 74.9 %copy-start.6 = (f32[320,128]{1,0:T(8,128)S(1)}, f32[320,128]{1,0:T(8,128)}, u32[]{:S(2)}) copy-start(f32[320,128]{1,0:T(8,128)} %param.19) | copy-start | bytes 491524
  130.5 52.4 %copy-start.2 = (f32[320,128]{1,0:T(8,128)}, f32[320,128]{1,0:T(8,128)S(1)}, u32[]{:S(2)}) copy-start(f32[320,128]{1,0:T(8,128)S(1)} %fusion.2) | copy-start | bytes 491524
Sparse Core Ops, SparseCore 0:
  133.0 46.2 all-gather.1
where the time goes:
time: 190 us
  blocking collectives  106 us (56%)
  waiting for transfers between devices  46.5 us (24%)
  between operations  16.3 us (9%)
  matrix products  11.8 us (6%)
  local copies, waits for them, and re-layouts  4.78 us (3%)
  other arithmetic  3.89 us (2%)
    all_gather x1, waiting for transfers between devices, turned_gather(): filled = lax.all_gather(both, axis, axis=0, tiled=True)  46.4 us
    all_to_all x1, blocking collectives, sent_to_all(): return lax.all_to_all(copies, axis, split_axis=0, concat_axis=0, tiled=True)  36.4 us
    psum x4, blocking collectives, by_axis(): array = lax.psum(array, axis)  33.1 us
    all_gather x1, blocking collectives, in_one_piece_2(): filled = lax.all_gather(both, axis, axis=dim, tiled=True)  21.7 us
    all_to_all x1, blocking collectives, sent_and_summed(): lax.all_to_all(blocks, axis, split_axis=0, concat_axis=0, tiled=True)  15.2 us
    dot_general x2, matrix products, shards(): jnp.dot(pairs[number][0], wholes[number], preferred_element_type=jnp.floa...  8.31 us
  transfers between devices with their start and end apart: 1, of which 1 were waited for; matrix products, arithmetic and copies ran while one was open for 0% of the time, Pallas kernels for 0%

commit v1 on v0

--- a/solution.py
+++ b/solution.py
@@ -59,7 +59,7 @@
 
 def by_axis(array, axes):
     for axis in axes:
-        array = lax.psum(array, axis)
+        array = jnp.sum(lax.all_gather(array, axis), axis=0)
     return array
 
 

time: 190 us -> 198 us (1.042)
  blocking collectives: 106 us -> 88.7 us
  waiting for transfers between devices: 46.5 us -> 57.4 us
  local copies, waits for them, and re-layouts: 4.78 us -> 13 us
  starting transfers between devices: 0.04 us -> 3.77 us
  other arithmetic: 3.89 us -> 6.32 us
    psum x4 -> x0, blocking collectives: 33.1 us -> none  [by_axis(): array = lax.psum(array, axis)]
    unnamed x0 -> x4, blocking collectives: none -> 30.3 us
    all_to_all x1 -> x0, blocking collectives: 15.2 us -> none  [sent_and_summed(): lax.all_to_all(blocks, axis, split_axis=0, concat_axis=0, tiled=True)]
    all_to_all x0 -> x1, waiting for transfers between devices: none -> 11.2 us  [sent_and_summed(): lax.all_to_all(blocks, axis, split_axis=0, concat_axis=0, tiled=True)]
    unnamed x26 -> x46, local copies, waits for them, and re-layouts: 0.83 us -> 8.16 us
    all_to_all x0 -> x1, starting transfers between devices: none -> 3.73 us  [sent_and_summed(): lax.all_to_all(blocks, axis, split_axis=0, concat_axis=0, tiled=True)]
    reduce_sum x0 -> x4, other arithmetic: none -> 2.41 us  [by_axis(): array = jnp.sum(lax.all_gather(array, axis), axis=0)]
  transfers between devices with their start and end apart: 1 -> 2, of which waited for: 1 -> 2; matrix products, arithmetic and copies ran while one was open for 0% -> 0% of each run, Pallas kernels for 0% -> 0%
where the time goes in v1:
time: 198 us; the launch traced here: 197 us
  blocking collectives  88.7 us (45%)
  waiting for transfers between devices  57.4 us (29%)
  between operations  16.3 us (8%)
  local copies, waits for them, and re-layouts  13 us (7%)
  matrix products  11.8 us (6%)
  other arithmetic  6.32 us (3%)
  starting transfers between devices  3.77 us (2%)
    all_gather x1, waiting for transfers between devices, turned_gather(): filled = lax.all_gather(both, axis, axis=0, tiled=True)  46.2 us
    all_to_all x1, blocking collectives, sent_to_all(): return lax.all_to_all(copies, axis, split_axis=0, concat_axis=0, tiled=True)  36.4 us
    unnamed x4, blocking collectives  30.3 us
    all_gather x1, blocking collectives, in_one_piece_2(): filled = lax.all_gather(both, axis, axis=dim, tiled=True)  21.9 us
    all_to_all x1, waiting for transfers between devices, sent_and_summed(): lax.all_to_all(blocks, axis, split_axis=0, concat_axis=0, tiled=True)  11.2 us
    dot_general x2, matrix products, shards(): jnp.dot(pairs[number][0], wholes[number], preferred_element_type=jnp.floa...  8.31 us
    unnamed x46, local copies, waits for them, and re-layouts  8.16 us
  transfers between devices with their start and end apart: 2, of which 2 were waited for; matrix products, arithmetic and copies ran while one was open for 0% of the time, Pallas kernels for 0%

profile of v1, /device:TPU:0, one launch (start us, length us, event | category | flops | bytes accessed | tf_op | source)
XLA Modules:
  0.0 197.2 jit_solution(12693672781650655608)
XLA Ops:
  7.2 1.0 pad_maximum_fusion.2
  8.4 36.4 %all_to_all.10 = bf16[16,128,512]{2,1,0:T(8,128)(2,1)S(1)} all-to-all(bf16[16,128,512]{2,1,0:T(8,128)(2,1)S(1)} %broadcast_in_dim.3), channel_id=1, replica_groups=mesh['fs_0'=4,'fs_1'=4,'tp_0'=4,'tp_1'=2] {'fs_0','fs_1'}, dimensions={0} | all-to-all | bytes 4194304 | tf_op jit(solution)/shard_map/all_to_all | solution.py:23
  44.8 5.9 %fusion.10 = (bf16[2048,256]{0,1:T(8,128)(2,1)S(1)}, f32[2048,256]{0,1:T(8,128)S(1)}) fusion(bf16[2048,2048]{1,0:T(8,128)(2,1)} %param.15, bf16[2048,512]{1,0:T(8,128)(2,1)S(1)} %bitcast.30), kind=kOutput, calls=%fused_computation.33 | convolution fusion | flops 2148007936 | bytes 12582912 | tf_op jit(solution)/shard_map/dot_general | solution.py:122
  50.8 2.4 %fusion.11 = (bf16[2048,256]{0,1:T(8,128)(2,1)S(1)}, f32[2048,256]{0,1:T(8,128)S(1)}) fusion(bf16[2048,2048]{1,0:T(8,128)(2,1)S(1)} %bitcast.33, bf16[2048,512]{1,0:T(8,128)(2,1)S(1)} %bitcast.31), kind=kOutput, calls=%fused_computation.34 | convolution fusion | flops 2148007936 | bytes 12582912 | tf_op jit(solution)/shard_map/dot_general | solution.py:122
  54.3 0.7 copy-done.1
  56.4 1.1 copy.22
  57.5 3.7 %all-to-all-start.1 = ((f32[16,16,640]{2,1,0:T(8,128)}), f32[16,16,640]{2,1,0:T(8,128)S(1)}, u32[]{:S(2)}, u32[]{:S(2)}) async-start(f32[16,16,640]{2,1,0:T(8,128)} %bitcast.3), calls=%async_computation.1 | async-start | bytes 1310720 | tf_op jit(solution)/shard_map/all_to_all | solution.py:47
  61.8 11.2 %all-to-all-done.1 = f32[16,16,640]{2,1,0:T(8,128)S(1)} async-done(((f32[16,16,640]{2,1,0:T(8,128)}), f32[16,16,640]{2,1,0:T(8,128)S(1)}, u32[]{:S(2)}, u32[]{:S(2)}) %all-to-all-start.1) | async-done | bytes 655392 | tf_op jit(solution)/shard_map/all_to_all | solution.py:47
  73.1 0.7 multiply_reduce_fusion
  75.1 0.8 dynamic-update-slice
  76.4 8.5 %all-reduce = f32[4]{0:T(128)S(1)} all-reduce(f32[4]{0:T(128)S(1)} %dynamic-update-slice), channel_id=1, replica_groups=mesh['fs_0'=4,'fs_1'=4,'tp_0'=4,'tp_1'=2] {'fs_0'}, use_global_device_ids=true, to_apply=%add | all-reduce | flops 4 | bytes 32
  85.5 1.4 dynamic-update-slice.1
  87.5 8.6 %all-reduce.1 = f32[4]{0:T(128)S(1)} all-reduce(f32[4]{0:T(128)S(1)} %dynamic-update-slice.1), channel_id=1, replica_groups=mesh['fs_0'=4,'fs_1'=4,'tp_0'=4,'tp_1'=2] {'fs_1'}, use_global_device_ids=true, to_apply=%add.1 | all-reduce | flops 4 | bytes 32
  96.7 1.4 dynamic-update-slice.2
  98.7 10.7 %all-reduce.2 = f32[4]{0:T(128)S(1)} all-reduce(f32[4]{0:T(128)S(1)} %dynamic-update-slice.2), channel_id=1, replica_groups=mesh['fs_0'=4,'fs_1'=4,'tp_0'=4,'tp_1'=2] {'tp_0'}, use_global_device_ids=true, to_apply=%add.2 | all-reduce | flops 4 | bytes 32
  110.0 1.4 dynamic-update-slice.3
  111.4 2.4 %all-reduce.3 = f32[2]{0:T(128)S(1)} all-reduce(f32[2]{0:T(128)S(1)} %dynamic-update-slice.3), channel_id=1, replica_groups=mesh['fs_0'=4,'fs_1'=4,'tp_0'=4,'tp_1'=2] {'tp_1'}, use_global_device_ids=true, to_apply=%add.3 | all-reduce | flops 2 | bytes 16
  115.2 0.7 divide_convert_fusion.1
  116.0 21.9 %all_gather.38 = bf16[256,640]{1,0:T(8,128)(2,1)S(1)} all-gather(bf16[16,640]{1,0:T(8,128)(2,1)S(1)} %pad_maximum_fusion.3), channel_id=1, replica_groups=mesh['fs_0'=4,'fs_1'=4,'tp_0'=4,'tp_1'=2] {'fs_0','fs_1'}, dimensions={0}, use_global_device_ids=true | all-gather | bytes 348160 | tf_op jit(solution)/shard_map/all_gather | solution.py:69
  138.3 1.0 fusion.7
  139.3 0.7 convert_bitcast_fusion
  140.0 0.7 pad_maximum_fusion.1
  140.7 46.2 %all-gather.2.cloned.1.call-done = bf16[2048,640]{0,1:T(8,128)(2,1)} async-done(((bf16[128,640]{0,1:T(8,128)(2,1)}), bf16[2048,640]{0,1:T(8,128)(2,1)}) %all-gather.2.cloned.1.call-update) | async-done | bytes 2621456 | tf_op jit(solution)/shard_map/all_gather | solution.py:77
  186.8 3.5 %slice_bitcast_fusion = (bf16[320,2048]{1,0:T(8,128)(2,1)}, bf16[2048,320]{0,1:T(8,128)(2,1)}) fusion(bf16[2048,640]{0,1:T(8,128)(2,1)} %all-gather.2.cloned.1.call-done), kind=kLoop, calls=%fused_computation.4 | loop fusion | bytes 5242880 | tf_op jit(solution)/shard_map/transpose | solution.py:81
  (57 shorter events, 7.8 us)
Async XLA Ops:
  7.2 46.0 %copy-start = (bf16[2048,320]{0,1:T(8,128)(2,1)S(1)}, bf16[2048,320]{0,1:T(8,128)(2,1)}, u32[]{:S(2)}) copy-start(bf16[2048,320]{0,1:T(8,128)(2,1)} %param.14) | copy-start | bytes 3932164
  8.4 42.4 %slice-start = ((s8[8388608]{0:T(1024)(128)(4,1)}), s8[4194304]{0:T(1024)(128)(4,1)S(1)}, s32[]{:S(2)}) async-start(s8[8388608]{0:T(1024)(128)(4,1)} %bitcast.32), calls=%async_computation.3 | async-start | bytes 8388608
  44.8 5.9 %slice-start.1 = ((s8[8388608]{0:T(1024)(128)(4,1)}), s8[4194304]{0:T(1024)(128)(4,1)S(1)}, s32[]{:S(2)}) async-start(s8[8388608]{0:T(1024)(128)(4,1)} %bitcast.32), calls=%async_computation.4 | async-start | bytes 8388608
  53.7 1.3 copy-start.1
  56.2 5.1 %copy-start.14 = (u32[128]{0:T(128)S(1)}, u32[128]{0:T(128)}, u32[]{:S(2)}) copy-start(u32[128]{0:T(128)} %constant.21) | copy-start | bytes 1540
  56.2 19.6 %copy-start.13 = (u32[128]{0:T(128)S(1)}, u32[128]{0:T(128)}, u32[]{:S(2)}) copy-start(u32[128]{0:T(128)} %constant.26) | copy-start | bytes 1540
  56.2 30.7 %copy-start.12 = (u32[128]{0:T(128)S(1)}, u32[128]{0:T(128)}, u32[]{:S(2)}) copy-start(u32[128]{0:T(128)} %constant.31) | copy-start | bytes 1540
  56.2 41.9 %copy-start.11 = (u32[128]{0:T(128)S(1)}, u32[128]{0:T(128)}, u32[]{:S(2)}) copy-start(u32[128]{0:T(128)} %constant.36) | copy-start | bytes 1540
  56.3 58.9 %copy-start.7 = (f32[16,320]{1,0:T(8,128)S(1)}, f32[16,320]{1,0:T(8,128)}, u32[]{:S(2)}) copy-start(f32[16,320]{1,0:T(8,128)} %param.21) | copy-start | bytes 61444
  56.3 58.9 %copy-start.8 = (f32[16,320]{1,0:T(8,128)S(1)}, f32[16,320]{1,0:T(8,128)}, u32[]{:S(2)}) copy-start(f32[16,320]{1,0:T(8,128)} %param.20) | copy-start | bytes 61444
  56.3 58.9 %copy-start.9 = (f32[16,320]{1,0:T(8,128)S(1)}, f32[16,320]{1,0:T(8,128)}, u32[]{:S(2)}) copy-start(f32[16,320]{1,0:T(8,128)} %param.23) | copy-start | bytes 61444
  56.3 58.9 %copy-start.10 = (f32[16,320]{1,0:T(8,128)S(1)}, f32[16,320]{1,0:T(8,128)}, u32[]{:S(2)}) copy-start(f32[16,320]{1,0:T(8,128)} %param.22) | copy-start | bytes 61444
  56.4 81.6 %copy-start.4 = (bf16[128,256]{1,0:T(8,128)(2,1)S(1)}, bf16[128,256]{1,0:T(8,128)(2,1)}, u32[]{:S(2)}) copy-start(bf16[128,256]{1,0:T(8,128)(2,1)} %param.17) | copy-start | bytes 196612
  56.4 81.9 %copy-start.3 = (bf16[128,256]{1,0:T(8,128)(2,1)S(1)}, bf16[128,256]{1,0:T(8,128)(2,1)}, u32[]{:S(2)}) copy-start(bf16[128,256]{1,0:T(8,128)(2,1)} %param.16) | copy-start | bytes 196612
  56.4 81.9 %copy-start.5 = (f32[128,320]{0,1:T(8,128)S(1)}, f32[128,320]{0,1:T(8,128)}, u32[]{:S(2)}) copy-start(f32[128,320]{0,1:T(8,128)} %param.18) | copy-start | bytes 491524
  57.5 81.8 %copy-start.6 = (f32[320,128]{1,0:T(8,128)S(1)}, f32[320,128]{1,0:T(8,128)}, u32[]{:S(2)}) copy-start(f32[320,128]{1,0:T(8,128)} %param.19) | copy-start | bytes 491524
  57.5 15.6 %all-to-all-start.1 = ((f32[16,16,640]{2,1,0:T(8,128)}), f32[16,16,640]{2,1,0:T(8,128)S(1)}, u32[]{:S(2)}, u32[]{:S(2)}) async-start(f32[16,16,640]{2,1,0:T(8,128)} %bitcast.3), calls=%async_computation.1 | async-start | bytes 1310720 | tf_op jit(solution)/shard_map/all_to_all | solution.py:47
  61.2 125.6 %all-gather.2.cloned.1.call-start = ((), (), s32[]{:S(2)}) async-start(), calls=%async_computation.2 | async-start | bytes 2785280 | tf_op jit(solution)/shard_map/all_gather | solution.py:77
  138.3 52.1 %copy-start.2 = (f32[320,128]{1,0:T(8,128)}, f32[320,128]{1,0:T(8,128)S(1)}, u32[]{:S(2)}) copy-start(f32[320,128]{1,0:T(8,128)S(1)} %fusion.2) | copy-start | bytes 491524
Sparse Core Ops, SparseCore 0:
  140.8 46.0 all-gather.1
